TPU v7x, 32 devices: a whole 2x2x4 slice. The times are simulated.
32 devices in a mesh: tp: 8 (over z, y), dp: 4 (over x, core).
Axes of the slice: x: 2, y: 2, z: 4, core: 2. Of those that a mesh axis runs over, the one named last changes fastest.
Arguments:
- tokens: bfloat16 [192, 8448], P('dp', 'tp'), may hold values from -6 to 6
- gains: float32 [2, 8448], replicated, may hold values from 0.1 to 1.9
- w_input: bfloat16 [2, 8448, 12288], P(None, 'dp', 'tp'), may hold values from -0.0625 to 0.0625
- w_gating: bfloat16 [2, 8448, 12288], P(None, 'dp', 'tp'), may hold values from -0.0625 to 0.0625
- w_output: bfloat16 [2, 12288, 8448], P(None, 'tp'), may hold values from -0.21875 to 0.21875
- decay_rate: float32 [2, 768, 64], P(None, 'tp'), may hold values from 0.05 to 2
- frequency: float32 [2, 768, 64], P(None, 'tp'), may hold values from -3 to 3
- log_step: float32 [2, 768], P(None, 'tp'), may hold values from -2.3 to 0
- in_real: float32 [2, 768, 64, 16], P(None, 'tp'), may hold values from -1 to 1
- in_imag: float32 [2, 768, 64, 16], P(None, 'tp'), may hold values from -1 to 1
- readout_real_matrix: float32 [2, 768, 16, 64], P(None, 'tp'), may hold values from -0.5 to 0.5
- readout_imag_matrix: float32 [2, 768, 16, 64], P(None, 'tp'), may hold values from -0.5 to 0.5
- skip_gain: float32 [2, 12288], P(None, 'tp'), may hold values from -4 to 4
- state_real: float32 [2, 192, 768, 64], P(None, 'dp', 'tp'), may hold values from -6 to 6
- state_imag: float32 [2, 192, 768, 64], P(None, 'dp', 'tp'), may hold values from -6 to 6
Outputs:
- mixed: bfloat16 [192, 8448], P('dp', 'tp')
- next_real: float32 [2, 192, 768, 64], P(None, 'dp', 'tp')
- next_imag: float32 [2, 192, 768, 64], P(None, 'dp', 'tp')
All inputs are finite; a program needn't handle non-finite values.
Results may differ from a plain program's by a relative error of at most 0.008.
Values may be sent and summed in bfloat16 or wider, within the bound.
A program may use at most 256 MiB of HBM per device.

v0:
```python
import jax
import jax.numpy as jnp
from jax import lax
from jax.sharding import PartitionSpec as P

GS = 16
LAYERS = 2


PRECISION_LEVEL = lax.Precision.HIGHEST


def collect(shard):
    return lax.all_gather(shard, "tp", axis=1, tiled=True)


def spread(partial_value):
    return lax.psum_scatter(partial_value, "tp", scatter_dimension=1, tiled=True)


def on_device(
    tokens,
    gains,
    w_input,
    w_gating,
    w_output,
    decay_rate,
    frequency,
    log_step,
    in_real,
    in_imag,
    readout_real_matrix,
    readout_imag_matrix,
    skip_gain,
    state_real,
    state_imag,
):
    width = tokens.shape[1]
    offset = lax.axis_index("tp") * width
    batch = tokens.shape[0]
    groups = decay_rate.shape[1]
    shard = tokens
    whole = collect(shard)
    outs_re = []
    outs_im = []
    for layer_params in range(LAYERS):
        xf = whole.astype(jnp.float32)
        meansq = jnp.mean(xf * xf, axis=1, keepdims=True)
        inverse = lax.rsqrt(meansq + 1e-06)
        scaled = (xf * gains[layer_params][None, :]).astype(jnp.bfloat16)
        drive = jnp.dot(
            scaled,
            lax.all_gather(w_input[layer_params], "dp", axis=0, tiled=True),
            preferred_element_type=jnp.float32,
        )
        gate = jnp.dot(
            scaled,
            lax.all_gather(w_gating[layer_params], "dp", axis=0, tiled=True),
            preferred_element_type=jnp.float32,
        )
        drive = drive * inverse
        gate = gate * inverse
        step = jnp.exp(log_step[layer_params])[:, None]
        lam_re = -decay_rate[layer_params]
        lam_im = frequency[layer_params]
        magnitude = jnp.exp(lam_re * step)
        angle = lam_im * step
        abar_re = magnitude * jnp.cos(angle)
        abar_im = magnitude * jnp.sin(angle)
        denom = lam_re * lam_re + lam_im * lam_im
        num_re = abar_re - 1.0
        zoh_re = (num_re * lam_re + abar_im * lam_im) / denom
        zoh_im = (abar_im * lam_re - num_re * lam_im) / denom
        bbar_re = (
            zoh_re[..., None] * in_real[layer_params] - zoh_im[..., None] * in_imag[layer_params]
        )
        bbar_im = (
            zoh_re[..., None] * in_imag[layer_params] + zoh_im[..., None] * in_real[layer_params]
        )
        grouped = drive.reshape(batch, groups, GS)
        push_re = jnp.einsum("bgc,gpc->bgp", grouped, bbar_re, precision=PRECISION_LEVEL)
        push_im = jnp.einsum("bgc,gpc->bgp", grouped, bbar_im, precision=PRECISION_LEVEL)
        old_re = state_real[layer_params]
        old_im = state_imag[layer_params]
        updated_real = abar_re[None] * old_re - abar_im[None] * old_im + push_re
        updated_imag = abar_re[None] * old_im + abar_im[None] * old_re + push_im
        readout_output = jnp.einsum(
            "zju,jiu->zji",
            updated_real,
            readout_real_matrix[layer_params],
            precision=PRECISION_LEVEL,
        ) - jnp.einsum(
            "zju,jiu->zji",
            updated_imag,
            readout_imag_matrix[layer_params],
            precision=PRECISION_LEVEL,
        )
        readout_output = (
            readout_output + skip_gain[layer_params].reshape(groups, GS)[None] * grouped
        )
        gated = (
            jax.nn.gelu(readout_output.reshape(batch, groups * GS)) * jax.nn.sigmoid(gate)
        ).astype(jnp.bfloat16)
        partial_value = jnp.dot(gated, w_output[layer_params], preferred_element_type=jnp.float32)
        outs_re.append(updated_real)
        outs_im.append(updated_imag)
        if layer_params + 1 < LAYERS:
            summed = lax.psum(partial_value, "tp")
            whole = (xf + summed).astype(jnp.bfloat16)
        else:
            own = lax.dynamic_slice_in_dim(whole, offset, width, 1)
            shard = (own.astype(jnp.float32) + spread(partial_value)).astype(jnp.bfloat16)
    return (shard, jnp.stack(outs_re, axis=0), jnp.stack(outs_im, axis=0))


def solution(mesh):
    placed = (
        P("dp", "tp"),
        P(),
        P(None, "dp", "tp"),
        P(None, "dp", "tp"),
        P(None, "tp", None),
        P(None, "tp", None),
        P(None, "tp", None),
        P(None, "tp"),
        P(None, "tp", None, None),
        P(None, "tp", None, None),
        P(None, "tp", None, None),
        P(None, "tp", None, None),
        P(None, "tp"),
        P(None, "dp", "tp", None),
        P(None, "dp", "tp", None),
    )
    return jax.shard_map(
        on_device,
        mesh=mesh,
        in_specs=placed,
        out_specs=(P("dp", "tp"), P(None, "dp", "tp", None), P(None, "dp", "tp", None)),
        check_vma=False,
    )
```

profile of v0, /device:TPU:15, one launch (start us, length us, event | category | flops | bytes accessed | tf_op | source)
XLA Modules:
  0.0 893.0 jit_solution(3569177894118164036)
XLA Ops:
  7.2 10.3 %fusion.143 = (bf16[1,2112,1536]{2,1,0:T(8,128)(2,1)}, bf16[1,2112,1536]{2,1,0:T(8,128)(2,1)}) fusion(bf16[2,2112,1536]{2,1,0:T(8,128)(2,1)} %param.17), kind=kLoop, calls=%fused_computation.162 | loop fusion | bytes 25952256 | tf_op jit(solution)/shard_map/slice | solution.py:53
  17.6 10.9 %fusion.144 = (bf16[1,2112,1536]{2,1,0:T(8,128)(2,1)}, bf16[1,2112,1536]{2,1,0:T(8,128)(2,1)}) fusion(bf16[2,2112,1536]{2,1,0:T(8,128)(2,1)} %param.18), kind=kLoop, calls=%fused_computation.163 | loop fusion | bytes 25952256 | tf_op jit(solution)/shard_map/slice | solution.py:58
  33.4 25.6 %all-gather.4 = bf16[8,1056,48]{1,2,0:T(8,128)(2,1)S(1)} all-gather(bf16[1,1056,48]{1,2,0:T(8,128)(2,1)S(1)} %bitcast.329), channel_id=1, replica_groups=mesh['tp'=8,'dp'=4] {'tp'}, dimensions={0}, use_global_device_ids=true | all-gather | bytes 912384 | tf_op jit(solution)/shard_map/all_gather | solution.py:14
  61.9 3.5 fusion.145
  67.3 3.5 fusion.146
  72.7 2.2 fusion.148
  77.4 2.1 fusion.147
  83.1 94.3 %all-gather.10.cloned.1.call-done = bf16[1,8448,1536]{2,1,0:T(8,128)(2,1)} async-done(((bf16[1,2112,1536]{2,1,0:T(8,128)(2,1)}), bf16[1,8448,1536]{2,1,0:T(8,128)(2,1)}) %all-gather.10.cloned.1.call-update) | async-done | bytes 25952272 | tf_op jit(solution)/shard_map/all_gather | solution.py:53
  177.4 10.8 %fusion.21 = f32[48,1536]{1,0:T(8,128)S(1)} fusion(bf16[1,8448,1536]{2,1,0:T(8,128)(2,1)} %all-gather.10.cloned.1.call-done, f32[8448,48]{0,1:T(8,128)S(1)} %reshape.330, f32[8448]{0:T(1024)S(1)} %get-tuple-element.13, f32[48]{0:T(128)S(1)} %add_rsqrt_fusion.1), kind=kOutput, calls=%fused_computation.33 | convolution fusion | flops 1246593024 | bytes 27903168 | tf_op jit(solution)/shard_map/dot_general | solution.py:51
  188.5 6.9 bitcast_add_fusion.3
  195.5 3.8 fusion.86
  199.3 3.9 bitcast_add_fusion.2
  203.3 3.8 fusion.81
  207.4 130.8 %all-gather.12.cloned.1.call-done = bf16[1,8448,1536]{2,1,0:T(8,128)(2,1)} async-done(((bf16[1,2112,1536]{2,1,0:T(8,128)(2,1)}), bf16[1,8448,1536]{2,1,0:T(8,128)(2,1)}) %all-gather.12.cloned.1.call-update) | async-done | bytes 25952272 | tf_op jit(solution)/shard_map/all_gather | solution.py:58
  338.1 20.3 %fusion.6 = f32[48,8448]{1,0:T(8,128)} fusion(bf16[2,1536,8448]{2,1,0:T(8,128)(2,1)} %param.19, bf16[1,8448,1536]{2,1,0:T(8,128)(2,1)} %all-gather.12.cloned.1.call-done, f32[48,1536]{1,0:T(8,128)S(1)} %copy.90, f32[8448,48]{0,1:T(8,128)S(1)} %reshape.330, f32[8448]{0:T(1024)S(1)} %get-tuple-element.13, f32[48]{0:T(128)S(1)} %add_rsqrt_fusion.1), kind=kOutput, calls=%fused_computation.6 | convolution fusion | flops 2493259776 | bytes 55477440 | tf_op jit(solution)/shard_map/dot_general | solution.py:104
  359.7 2.3 copy.98
  362.8 1.9 copy.113
  364.7 3.1 copy.114
  372.3 76.4 %all-reduce.2.cloned.1.call-done = f32[48,8448]{1,0:T(8,128)} async-done(((f32[48,8448]{1,0:T(8,128)}), f32[48,8448]{1,0:T(8,128)}) %all-reduce.2.cloned.1.call-update) | async-done | bytes 1622032 | tf_op jit(solution)/shard_map/psum | solution.py:108
  450.4 158.6 %all-gather.14.cloned.1.call-done = bf16[1,8448,1536]{2,1,0:T(8,128)(2,1)} async-done(((bf16[1,2112,1536]{2,1,0:T(8,128)(2,1)}), bf16[1,8448,1536]{2,1,0:T(8,128)(2,1)}) %all-gather.14.cloned.1.call-update) | async-done | bytes 25952272 | tf_op jit(solution)/shard_map/all_gather | solution.py:53
  609.0 11.1 %fusion.42 = f32[48,1536]{1,0:T(8,128)S(1)} fusion(bf16[1,8448,1536]{2,1,0:T(8,128)(2,1)} %all-gather.14.cloned.1.call-done, bf16[48,8448]{1,0:T(8,128)(2,1)S(1)} %get-tuple-element.17, f32[8448]{0:T(1024)S(1)} %copy-done.31, f32[48]{0:T(128)S(1)} %add_rsqrt_fusion), kind=kOutput, calls=%fused_computation.40 | convolution fusion | flops 1246998528 | bytes 27092160 | tf_op jit(solution)/shard_map/dot_general | solution.py:51
  620.4 6.9 bitcast_add_fusion.1
  627.4 3.8 fusion.83
  631.2 4.0 bitcast_add_fusion
  635.3 4.0 fusion.79
  639.5 130.0 %all-gather.16.cloned.1.call-done = bf16[1,8448,1536]{2,1,0:T(8,128)(2,1)} async-done(((bf16[1,2112,1536]{2,1,0:T(8,128)(2,1)}), bf16[1,8448,1536]{2,1,0:T(8,128)(2,1)}) %all-gather.16.cloned.1.call-update) | async-done | bytes 25952272 | tf_op jit(solution)/shard_map/all_gather | solution.py:58
  769.6 22.6 %fusion.14 = f32[8448,48]{1,0:T(8,128)} fusion(bf16[2,1536,8448]{2,1,0:T(8,128)(2,1)} %param.19, bf16[1,8448,1536]{2,1,0:T(8,128)(2,1)} %all-gather.16.cloned.1.call-done, bf16[48,8448]{1,0:T(8,128)(2,1)S(1)} %copy-done.12, f32[8448]{0:T(1024)S(1)} %copy-done.31, f32[48,1536]{1,0:T(8,128)S(1)} %copy.104, f32[48]{0:T(128)S(1)} %add_rsqrt_fusion), kind=kOutput, calls=%fused_computation.14 | convolution fusion | flops 2493665280 | bytes 54666432
  793.8 4.1 pad_maximum_fusion.1
  797.9 5.9 copy.106
  803.9 4.1 pad_maximum_fusion
  808.0 5.8 copy.105
  813.7 69.1 %reduce-scatter.4.cloned.1.call-done = f32[1056,48]{1,0:T(8,128)} async-done(((f32[8448,48]{1,0:T(8,128)}), f32[1056,48]{1,0:T(8,128)}) %reduce-scatter.4.cloned.1.call-update) | async-done | bytes 202768
  (127 shorter events, 31.6 us)
Async XLA Ops:
  7.2 170.2 %all-gather.10.cloned.1.call-start = ((), (), s32[]{:S(2)}) async-start(), calls=%async_computation.2 | async-start | bytes 32440320 | tf_op jit(solution)/shard_map/all_gather | solution.py:53
  17.5 320.6 %all-gather.12.cloned.1.call-start = ((), (), s32[]{:S(2)}) async-start(), calls=%async_computation.3 | async-start | bytes 32440320 | tf_op jit(solution)/shard_map/all_gather | solution.py:58
  28.5 420.1 %all-reduce.2.cloned.1.call-start = ((), (), s32[]{:S(2)}) async-start(), calls=%async_computation.1 | async-start | bytes 3244032 | tf_op jit(solution)/shard_map/psum | solution.py:108
  76.1 4.7 copy-start.39
  76.1 6.0 copy-start.37
  177.4 11.1 %copy-start.13 = (f32[96,64,16]{1,2,0:T(8,128)S(1)}, f32[96,64,16]{1,2,0:T(8,128)}, u32[]{:S(2)}) copy-start(f32[96,64,16]{1,2,0:T(8,128)} %copy.82) | copy-start | bytes 1179652
  188.5 7.0 copy-start.19
  188.5 10.8 %copy-start.9 = (f32[1,48,96,64]{3,1,2,0:T(8,128)S(1)}, f32[1,48,96,64]{3,1,2,0:T(8,128)}, u32[]{:S(2)}) copy-start(f32[1,48,96,64]{3,1,2,0:T(8,128)} %copy.110) | copy-start | bytes 3538948
  195.5 7.8 copy-start
  195.5 3.8 copy-start.7
  195.5 3.8 copy-start.15
  195.5 3.8 copy-start.26
  195.5 3.8 copy-start.27
  199.3 4.0 copy-start.17
  199.3 4.0 copy-start.33
  358.4 250.5 %all-gather.14.cloned.1.call-start = ((), (), s32[]{:S(2)}) async-start(), calls=%async_computation.4 | async-start | bytes 32440320 | tf_op jit(solution)/shard_map/all_gather | solution.py:53
  359.0 410.5 %all-gather.16.cloned.1.call-start = ((), (), s32[]{:S(2)}) async-start(), calls=%async_computation.5 | async-start | bytes 32440320 | tf_op jit(solution)/shard_map/all_gather | solution.py:58
  359.6 523.2 %reduce-scatter.4.cloned.1.call-start = ((), (), s32[]{:S(2)}) async-start(), calls=%async_computation.6 | async-start | bytes 4866048
  364.7 4.4 copy-start.22
  364.7 5.6 copy-start.23
  371.6 237.4 %copy-start.31 = (f32[8448]{0:T(1024)S(1)}, f32[8448]{0:T(1024)}, u32[]{:S(2)}) copy-start(f32[8448]{0:T(1024)} %get-tuple-element.12) | copy-start | bytes 101380
  450.4 158.6 %copy-start.11 = (bf16[48,8448]{1,0:T(8,128)(2,1)}, bf16[48,8448]{1,0:T(8,128)(2,1)S(1)}, u32[]{:S(2)}) copy-start(bf16[48,8448]{1,0:T(8,128)(2,1)S(1)} %get-tuple-element.17) | copy-start | bytes 2433028
  609.0 11.4 %copy-start.6 = (f32[1,48,96,64]{3,1,2,0:T(8,128)S(1)}, f32[1,48,96,64]{3,1,2,0:T(8,128)}, u32[]{:S(2)}) copy-start(f32[1,48,96,64]{3,1,2,0:T(8,128)} %copy.113) | copy-start | bytes 3538948
  620.4 6.9 copy-start.18
  627.4 7.9 copy-start.4
  627.4 3.8 copy-start.8
  627.4 3.8 copy-start.14
  631.2 4.0 copy-start.16
  631.2 4.0 copy-start.32
  635.2 4.1 copy-start.5
  635.3 134.3 %copy-start.12 = (bf16[48,8448]{1,0:T(8,128)(2,1)S(1)}, bf16[48,8448]{1,0:T(8,128)(2,1)}, u32[]{:S(2)}) copy-start(bf16[48,8448]{1,0:T(8,128)(2,1)} %copy-done.11) | copy-start | bytes 2433028
  797.9 5.9 copy-start.1
  (15 other events, 38.2 us)
Sparse Core Ops, SparseCore 0:
  17.6 159.7 all-gather.9
  179.0 159.1 all-gather.11
  358.6 90.0 all-reduce.1
  450.1 158.8 all-gather.13
  610.4 159.1 all-gather.15
  792.3 90.5 reduce-scatter.3
where the time goes:
time: 902 us; the launch traced here: 893 us
  waiting for transfers between devices  660 us (73%)
  matrix products  102 us (11%)
  local copies, waits for them, and re-layouts  75.6 us (8%)
  blocking collectives  25.6 us (3%)
  between operations  15 us (2%)
  other arithmetic  14.3 us (2%)
    all_gather x2, waiting for transfers between devices, on_device(): lax.all_gather(w_gating[layer_params], 'dp', axis=0, tiled=True)  261 us
    all_gather x2, waiting for transfers between devices, on_device(): lax.all_gather(w_input[layer_params], 'dp', axis=0, tiled=True)  253 us
    psum x1, waiting for transfers between devices, on_device(): summed = lax.psum(partial_value, 'tp')  76.4 us
    unnamed x7, waiting for transfers between devices  70.2 us
    unnamed x93, local copies, waits for them, and re-layouts  30.4 us
    all_gather x1, blocking collectives, collect(): return lax.all_gather(shard, 'tp', axis=1, tiled=True)  25.6 us
    unnamed x1, matrix products  22.6 us
    dot_general x2, matrix products, on_device(): jnp.dot(scaled, lax.all_gather(w_input[layer_params], 'dp', axis=0, tiled...  22 us
  transfers between devices with their start and end apart: 6, of which 6 were waited for; matrix products, arithmetic and copies ran while one was open for 15% of the time, Pallas kernels for 0%

commit v1 on v0

v1 whole, which is shorter than its diff:
```python
import functools

import jax
import jax.numpy as jnp
from jax import lax
from jax.experimental import pallas as pl
from jax.experimental.pallas import tpu as pltpu
from jax.sharding import PartitionSpec as P

GS = 16
LAYERS = 2
MESH = pl.DeviceIdType.MESH
ANY = pl.BlockSpec(memory_space=pl.ANY)


def exchange_kernel(axis, n, count, *refs):
    ins, outs = refs[:count], refs[count : 2 * count]
    send, recv, local = refs[2 * count :]
    me = lax.axis_index(axis)
    barrier = pltpu.get_barrier_semaphore()
    for i in range(1, n):
        pl.semaphore_signal(
            barrier, inc=1, device_id={axis: lax.rem(me + i, n)}, device_id_type=MESH
        )
    own = [
        pltpu.make_async_copy(ins[k].at[me], outs[k].at[me], local.at[k]) for k in range(count)
    ]
    for copy in own:
        copy.start()
    pl.semaphore_wait(barrier, n - 1)
    copies = []
    for i in range(1, n):
        peer = lax.rem(me + i, n)
        for k in range(count):
            copy = pltpu.make_async_remote_copy(
                src_ref=ins[k].at[peer],
                dst_ref=outs[k].at[me],
                send_sem=send.at[k, i],
                recv_sem=recv.at[k, i],
                device_id={axis: peer},
                device_id_type=MESH,
            )
            copy.start()
            copies.append((i, k, copy))
    for copy in own:
        copy.wait()
    for i, k, copy in copies:
        copy.wait_send()
        source = lax.rem(me + n - i, n)
        pltpu.make_async_remote_copy(
            src_ref=ins[k].at[source],
            dst_ref=outs[k].at[source],
            send_sem=send.at[k, i],
            recv_sem=recv.at[k, i],
            device_id={axis: source},
            device_id_type=MESH,
        ).wait_recv()


def exchange(arrays, axis, n, ident):
    count = len(arrays)
    return pl.pallas_call(
        functools.partial(exchange_kernel, axis, n, count),
        out_shape=[jax.ShapeDtypeStruct(a.shape, a.dtype) for a in arrays],
        in_specs=[ANY] * count,
        out_specs=[ANY] * count,
        scratch_shapes=[
            pltpu.SemaphoreType.DMA((count, n)),
            pltpu.SemaphoreType.DMA((count, n)),
            pltpu.SemaphoreType.DMA((count,)),
        ],
        compiler_params=pltpu.CompilerParams(collective_id=ident, has_side_effects=True),
        name=f"exchange_{axis}_{ident}",
    )(*arrays)


def gather_kernel(tp, dp, x_ref, out_ref, send, recv):
    q = tp // dp
    t = lax.axis_index("tp")
    d = lax.axis_index("dp")
    group = t // q
    slot = lax.rem(t, q) * dp + d
    barrier = pltpu.get_barrier_semaphore()
    for h in range(q):
        for r in range(dp):
            source = d * q + h
            pl.semaphore_signal(
                barrier, inc=1, device_id={"tp": source, "dp": r}, device_id_type=MESH
            )

    pl.semaphore_wait(barrier, tp)

    def remote(i, index):
        return pltpu.make_async_remote_copy(
            src_ref=x_ref,
            dst_ref=out_ref.at[index],
            send_sem=send.at[i],
            recv_sem=recv.at[index],
            device_id={"tp": lax.rem(t + i, tp), "dp": group},
            device_id_type=MESH,
        )

    home = group == d

    @pl.when(home)
    def _():
        pltpu.make_async_copy(x_ref, out_ref.at[slot], recv.at[slot]).start()

    @pl.when(jnp.logical_not(home))
    def _():
        remote(0, slot).start()

    for i in range(1, tp):
        remote(i, slot).start()
    for i in range(1, tp):
        remote(i, slot).wait_send()

    @pl.when(jnp.logical_not(home))
    def _():
        remote(0, slot).wait_send()

    for index in range(tp):
        pltpu.make_async_copy(x_ref, out_ref.at[index], recv.at[index]).wait()


def gather(x, tp, dp, ident):
    return pl.pallas_call(
        functools.partial(gather_kernel, tp, dp),
        out_shape=jax.ShapeDtypeStruct((tp,) + x.shape, x.dtype),
        in_specs=[ANY],
        out_specs=ANY,
        scratch_shapes=[pltpu.SemaphoreType.DMA((tp,)), pltpu.SemaphoreType.DMA((tp,))],
        compiler_params=pltpu.CompilerParams(collective_id=ident, has_side_effects=True),
        name=f"gather_{ident}",
    )(x)


def state_kernel(many, u_ref, are_ref, aim_ref, bre_ref, bim_ref, rre_ref, rim_ref, sre_ref, sim_ref, *rest):
    nre_ref, nim_ref, y_ref = rest[-3:]
    block, channels = u_ref.shape[0], u_ref.shape[1]
    states = are_ref.shape[1]
    cut = 4

    def body(step, carry):
        first = step * many
        for p in range(0, states, 8):
            rows = slice(p, p + 8)
            a_re, a_im = are_ref[0, rows, :], aim_ref[0, rows, :]
            new_re, new_im = [], []
            for b in range(many):
                o_re, o_im = sre_ref[0, first + b, rows, :], sim_ref[0, first + b, rows, :]
                new_re.append(a_re * o_re - a_im * o_im)
                new_im.append(a_re * o_im + a_im * o_re)
            for c in range(channels):
                b_re, b_im = bre_ref[0, c, rows, :], bim_ref[0, c, rows, :]
                for b in range(many):
                    u = u_ref[first + b, c : c + 1, :]
                    new_re[b] = new_re[b] + b_re * u
                    new_im[b] = new_im[b] + b_im * u
            for b in range(many):
                nre_ref[0, first + b, rows, :] = new_re[b]
                nim_ref[0, first + b, rows, :] = new_im[b]
        for c in range(0, channels, cut):
            total = [[None] * many for _ in range(cut)]
            for p in range(0, states, 8):
                rows = slice(p, p + 8)
                h_re = [nre_ref[0, first + b, rows, :] for b in range(many)]
                h_im = [nim_ref[0, first + b, rows, :] for b in range(many)]
                for j in range(cut):
                    r_re, r_im = rre_ref[0, c + j, rows, :], rim_ref[0, c + j, rows, :]
                    for b in range(many):
                        term = r_re * h_re[b] - r_im * h_im[b]
                        total[j][b] = term if p == 0 else total[j][b] + term
            for j in range(cut):
                for b in range(many):
                    y_ref[first + b, c + j : c + j + 1, :] = jnp.sum(
                        total[j][b], axis=0, keepdims=True
                    )
        return carry

    lax.fori_loop(0, block // many, body, 0)


def state_step(layer, u, a_re, a_im, b_re, b_im, r_re, r_im, s_re, s_im, earlier):
    batch, channels, groups = u.shape
    states = a_re.shape[1]
    block = 8
    per_batch = pl.BlockSpec((block, channels, groups), lambda i: (i, 0, 0))
    eigen = pl.BlockSpec((1, states, groups), lambda i: (layer, 0, 0))
    matrix = pl.BlockSpec((1, channels, states, groups), lambda i: (layer, 0, 0, 0))
    state = pl.BlockSpec((1, block, states, groups), lambda i: (layer, i, 0, 0))
    specs = [per_batch, eigen, eigen, matrix, matrix, matrix, matrix, state, state]
    aliases = {}
    if earlier:
        aliases = {len(specs): 0, len(specs) + 1: 1}
    return pl.pallas_call(
        functools.partial(state_kernel, 4),
        grid=(batch // block,),
        out_shape=[
            jax.ShapeDtypeStruct(s_re.shape, jnp.float32),
            jax.ShapeDtypeStruct(s_im.shape, jnp.float32),
            jax.ShapeDtypeStruct(u.shape, jnp.float32),
        ],
        in_specs=specs + [ANY] * len(earlier),
        out_specs=[state, state, per_batch],
        input_output_aliases=aliases,
        name=f"state_{layer}",
    )(u, a_re, a_im, b_re, b_im, r_re, r_im, s_re, s_im, *earlier)


def on_device(
    tp,
    dp,
    tokens,
    gains,
    w_input,
    w_gating,
    w_output,
    decay_rate,
    frequency,
    log_step,
    in_real,
    in_imag,
    readout_real_matrix,
    readout_imag_matrix,
    skip_gain,
    state_real,
    state_imag,
):
    batch, width = tokens.shape
    groups, states = decay_rate.shape[1:]
    channels = groups * GS
    rows = w_input.shape[1]
    features = gains.shape[1]
    q = tp // dp
    d = lax.axis_index("dp")

    step = jnp.exp(log_step)[:, None, :]
    lam_re = -jnp.swapaxes(decay_rate, 1, 2)
    lam_im = jnp.swapaxes(frequency, 1, 2)
    magnitude = jnp.exp(lam_re * step)
    angle = lam_im * step
    abar_re = magnitude * jnp.cos(angle)
    abar_im = magnitude * jnp.sin(angle)
    denom = lam_re * lam_re + lam_im * lam_im
    num_re = abar_re - 1.0
    zoh_re = ((num_re * lam_re + abar_im * lam_im) / denom)[:, None]
    zoh_im = ((abar_im * lam_re - num_re * lam_im) / denom)[:, None]
    i_re = jnp.transpose(in_real, (0, 3, 2, 1))
    i_im = jnp.transpose(in_imag, (0, 3, 2, 1))
    bbar_re = zoh_re * i_re - zoh_im * i_im
    bbar_im = zoh_re * i_im + zoh_im * i_re
    r_re = jnp.transpose(readout_real_matrix, (0, 2, 3, 1))
    r_im = jnp.transpose(readout_imag_matrix, (0, 2, 3, 1))
    s_re = jnp.swapaxes(state_real, 2, 3)
    s_im = jnp.swapaxes(state_imag, 2, 3)
    my_gains = lax.dynamic_slice_in_dim(gains, d * rows, rows, 1).reshape(LAYERS, q, 1, width)

    shard = tokens
    news = ()
    for layer in range(LAYERS):
        got = gather(shard, tp, dp, 3 * layer + 1).reshape(q, dp * batch, width)
        xf = got.astype(jnp.float32)
        squares = jnp.sum(xf * xf, axis=(0, 2))
        scaled = (xf * my_gains[layer]).astype(jnp.bfloat16)
        if q <= 2:
            scaled = jnp.concatenate([scaled[h] for h in range(q)], axis=1)
        else:
            scaled = jnp.swapaxes(scaled, 0, 1).reshape(dp * batch, rows)
        drive = jnp.dot(scaled, w_input[layer], preferred_element_type=jnp.float32)
        gate = jnp.dot(scaled, w_gating[layer], preferred_element_type=jnp.float32)
        drive, gate, squares = exchange(
            [
                drive.astype(jnp.bfloat16).reshape(dp, batch, channels),
                gate.astype(jnp.bfloat16).reshape(dp, batch, channels),
                jnp.broadcast_to(squares.reshape(dp, batch, 1), (dp, batch, 128)),
            ],
            "dp",
            dp,
            3 * layer + 2,
        )
        meansq = jnp.sum(squares, axis=0)[:, :1] / features
        inverse = lax.rsqrt(meansq + 1e-06)
        drive = jnp.sum(drive.astype(jnp.float32), axis=0) * inverse
        gate = jnp.sum(gate.astype(jnp.float32), axis=0) * inverse
        u = jnp.swapaxes(drive.reshape(batch, groups, GS), 1, 2)
        n_re, n_im, y = state_step(
            layer, u, abar_re, abar_im, bbar_re, bbar_im, r_re, r_im, s_re, s_im, news
        )
        news = (n_re, n_im)
        y = jnp.swapaxes(y, 1, 2).reshape(batch, channels) + skip_gain[layer][None] * drive
        z = (jax.nn.gelu(y) * jax.nn.sigmoid(gate)).astype(jnp.bfloat16)
        branch = jnp.dot(z, w_output[layer], preferred_element_type=jnp.float32)
        pieces = jnp.swapaxes(branch.astype(jnp.bfloat16).reshape(batch, tp, width), 0, 1)
        (pieces,) = exchange([pieces], "tp", tp, 3 * layer + 3)
        summed = jnp.sum(pieces.astype(jnp.float32), axis=0)
        shard = (shard.astype(jnp.float32) + summed).astype(jnp.bfloat16)
    return shard, jnp.swapaxes(news[0], 2, 3), jnp.swapaxes(news[1], 2, 3)


def solution(mesh):
    placed = (
        P("dp", "tp"),
        P(),
        P(None, "dp", "tp"),
        P(None, "dp", "tp"),
        P(None, "tp", None),
        P(None, "tp", None),
        P(None, "tp", None),
        P(None, "tp"),
        P(None, "tp", None, None),
        P(None, "tp", None, None),
        P(None, "tp", None, None),
        P(None, "tp", None, None),
        P(None, "tp"),
        P(None, "dp", "tp", None),
        P(None, "dp", "tp", None),
    )
    return jax.shard_map(
        functools.partial(on_device, mesh.shape["tp"], mesh.shape["dp"]),
        mesh=mesh,
        in_specs=placed,
        out_specs=(P("dp", "tp"), P(None, "dp", "tp", None), P(None, "dp", "tp", None)),
        check_vma=False,
    )
```

time: 902 us -> 235 us (0.26)
  waiting for transfers between devices: 660 us -> 0 us
  Pallas kernels: 0 us -> 154 us
  matrix products: 102 us -> 40.1 us
  local copies, waits for them, and re-layouts: 75.6 us -> 14.7 us
  blocking collectives: 25.6 us -> 0 us
  between operations: 15 us -> 0.94 us
  other arithmetic: 14.3 us -> 24 us
    all_gather x4 -> x0, waiting for transfers between devices: 514 us -> none  [the longest x2 261 us: on_device(): lax.all_gather(w_gating[layer_params], 'dp', axis=0, tiled=True)]
    pallas_call x0 -> x8, Pallas kernels: none -> 154 us  [the longest x4 88 us: exchange(): pl.pallas_call(functools.partial(exchange_kernel, axis, n, count), out_sh...]
    psum x1 -> x0, waiting for transfers between devices: 76.4 us -> none  [on_device(): summed = lax.psum(partial_value, 'tp')]
    unnamed x7 -> x0, waiting for transfers between devices: 70.2 us -> none
    dot_general x11 -> x6, matrix products: 79.3 us -> 40.1 us  [the longest x2 22 us: on_device(): branch = jnp.dot(z, w_output[layer], preferred_element_type=jnp.float32)]
    slice x8 -> x2, local copies, waits for them, and re-layouts: 33.8 us -> 1.74 us  [the longest x1 0.92 us: on_device(): scaled = (xf * my_gains[layer]).astype(jnp.bfloat16)]
    unnamed x93 -> x10, local copies, waits for them, and re-layouts: 30.4 us -> 1.35 us
    all_gather x1 -> x0, blocking collectives: 25.6 us -> none  [collect(): return lax.all_gather(shard, 'tp', axis=1, tiled=True)]
  transfers between devices with their start and end apart: 6 -> 0, of which waited for: 6 -> 0; matrix products, arithmetic and copies ran while one was open for 15% -> 0% of each run, Pallas kernels for 0% -> 0%
where the time goes in v1:
time: 235 us; the launch traced here: 234 us
  Pallas kernels  154 us (66%)
  matrix products  40.1 us (17%)
  other arithmetic  24 us (10%)
  local copies, waits for them, and re-layouts  14.7 us (6%)
    pallas_call x4, Pallas kernels, exchange(): pl.pallas_call(functools.partial(exchange_kernel, axis, n, count), out_sh...  88 us
    pallas_call x2, Pallas kernels, gather(): pl.pallas_call(functools.partial(gather_kernel, tp, dp), out_shape=jax.Sh...  45.3 us
    dot_general x2, matrix products, on_device(): branch = jnp.dot(z, w_output[layer], preferred_element_type=jnp.float32)  22 us
    pallas_call x2, Pallas kernels, state_step(): pl.pallas_call(functools.partial(state_kernel, 4), grid=(batch // block,)...  20.9 us
    dot_general x2, matrix products, on_device(): gate = jnp.dot(scaled, w_gating[layer], preferred_element_type=jnp.float32)  10.6 us
    dot_general x2, matrix products, on_device(): drive = jnp.dot(scaled, w_input[layer], preferred_element_type=jnp.float32)  7.55 us
    reshape x4, local copies, waits for them, and re-layouts, on_device(): branch.astype(jnp.bfloat16).reshape(batch, tp, width)  5.01 us

profile of v1, /device:TPU:15, one launch (start us, length us, event | category | flops | bytes accessed | tf_op | source)
XLA Modules:
  0.0 234.0 jit_solution(16361997349156199498)
XLA Ops:
  3.5 1.8 fusion.59
  5.4 22.5 %gather_1.1 = bf16[8,48,1056]{2,1,0:T(8,128)(2,1)} custom-call(bf16[48,1056]{1,0:T(8,128)(2,1)} %x_ref.1), custom_call_target="tpu_custom_call" | custom-call | tf_op jit(solution)/shard_map/gather_1/pallas_call | solution.py:127
  27.9 1.4 multiply_reduce_fusion.1
  30.3 1.3 convert_element_type.112
  31.7 5.3 %fusion.27 = bf16[192,1536]{1,0:T(8,128)(2,1)} fusion(bf16[2,2112,1536]{2,1,0:T(8,128)(2,1)} %param.18, bf16[192,1056]{1,0:T(8,128)(2,1)S(1)} %get-tuple-element.36, bf16[192,1056]{1,0:T(8,128)(2,1)S(1)} %get-tuple-element.35), kind=kOutput, calls=%fused_computation.21 | convolution fusion | flops 1247625216 | bytes 7888896 | tf_op jit(solution)/shard_map/dot_general | solution.py:271
  37.1 1.3 copy-done.4
  38.4 2.4 %fusion.24 = bf16[192,1536]{1,0:T(8,128)(2,1)} fusion(bf16[2,2112,1536]{2,1,0:T(8,128)(2,1)S(1)} %copy-done.4, bf16[192,1056]{1,0:T(8,128)(2,1)S(1)} %get-tuple-element.36, bf16[192,1056]{1,0:T(8,128)(2,1)S(1)} %get-tuple-element.35), kind=kOutput, calls=%fused_computation.20 | convolution fusion | flops 1247625216 | bytes 7962624 | tf_op jit(solution)/shard_map/dot_general | solution.py:270
  40.8 21.0 %exchange_dp_2.1 = (bf16[4,48,1536]{2,1,0:T(8,128)(2,1)}, bf16[4,48,1536]{2,1,0:T(8,128)(2,1)}, f32[4,48,128]{2,1,0:T(8,128)}) custom-call(bf16[4,48,1536]{2,1,0:T(8,128)(2,1)} %bitcast.178, bf16[4,48,1536]{2,1,0:T(8,128)(2,1)} %bitcast.177, f32[4,48,128]{2,1,0:T(8,128)} %broadcast_in_dim.18.refs_2_), custom_call_target="tpu_custom_call" | custom-call | tf_op jit(solution)/shard_map/exchange_dp_2/pallas_call | solution.py:62
  61.8 1.5 convert_reduce_fusion.4
  65.7 3.2 %fusion.39 = (f32[2,16,64,96]{3,2,1,0:T(8,128)}, f32[2,16,64,96]{3,2,1,0:T(8,128)}) fusion(f32[2,96,64,16]{1,3,2,0:T(8,128)S(1)} %copy-done, f32[2,96,64,16]{1,3,2,0:T(8,128)} %param.23, f32[2,64,96]{2,1,0:T(8,128)S(1)} %get-tuple-element.39, f32[2,64,96]{2,1,0:T(8,128)S(1)} %get-tuple-element.37), kind=kLoop, calls=%fused_computation.39 | loop fusion | flops 1179648 | bytes 3244032 | tf_op jit(solution)/shard_map/add | solution.py:252
  69.0 10.5 %state_0.1 = (f32[2,48,64,96]{3,2,1,0:T(8,128)}, f32[2,48,64,96]{3,2,1,0:T(8,128)}, f32[48,16,96]{2,1,0:T(8,128)}) custom-call(f32[48,16,96]{2,1,0:T(8,128)} %multiply_bitcast_fusion.1.u_ref, f32[2,64,96]{2,1,0:T(8,128)} %get-tuple-element.40.are_ref, f32[2,64,96]{2,1,0:T(8,128)} %get-tuple-element.38.aim_ref, f32[2,16,64,96]{3,2,1,0:T(8,128)} %get-tuple-element.32.bre_ref, ...), custom_call_target="tpu_custom_call" | custom-call | tf_op jit(solution)/shard_map/state_0/pallas_call | solution.py:196
  79.5 1.3 fusion.48
  81.2 10.9 %fusion.6 = bf16[48,8448]{1,0:T(8,128)(2,1)S(1)} fusion(bf16[48,1536]{0,1:T(8,128)(2,1)S(1)} %bitcast.175, bf16[2,1536,8448]{2,1,0:T(8,128)(2,1)} %param.19), kind=kOutput, calls=%fused_computation.6 | convolution fusion | flops 1246113792 | bytes 26910720 | tf_op jit(solution)/shard_map/dot_general | solution.py:293
  92.1 1.5 reshape.100
  93.6 1.0 copy.91
  94.6 23.4 %exchange_tp_3.1 = bf16[8,48,1056]{2,1,0:T(8,128)(2,1)} custom-call(bf16[8,48,1056]{2,1,0:T(8,128)(2,1)} %bitcast.167), custom_call_target="tpu_custom_call" | custom-call | tf_op jit(solution)/shard_map/exchange_tp_3/pallas_call | solution.py:62
  118.0 1.3 convert_reduce_fusion.1
  120.0 22.7 %gather_4.1 = bf16[8,48,1056]{2,1,0:T(8,128)(2,1)} custom-call(bf16[48,1056]{1,0:T(8,128)(2,1)} %add_convert_fusion.1.x_ref), custom_call_target="tpu_custom_call" | custom-call | tf_op jit(solution)/shard_map/gather_4/pallas_call | solution.py:127
  142.7 1.4 multiply_reduce_fusion
  145.1 1.3 convert_element_type.113
  146.6 5.2 %fusion.33 = bf16[192,1536]{1,0:T(8,128)(2,1)} fusion(bf16[2,2112,1536]{2,1,0:T(8,128)(2,1)} %param.18, bf16[192,1056]{1,0:T(8,128)(2,1)S(1)} %get-tuple-element.34, bf16[192,1056]{1,0:T(8,128)(2,1)S(1)} %get-tuple-element.33), kind=kOutput, calls=%fused_computation.23 | convolution fusion | flops 1247625216 | bytes 7888896 | tf_op jit(solution)/shard_map/dot_general | solution.py:271
  151.8 5.2 %fusion.30 = bf16[192,1536]{1,0:T(8,128)(2,1)} fusion(bf16[2,2112,1536]{2,1,0:T(8,128)(2,1)} %param.17, bf16[192,1056]{1,0:T(8,128)(2,1)S(1)} %get-tuple-element.34, bf16[192,1056]{1,0:T(8,128)(2,1)S(1)} %get-tuple-element.33), kind=kOutput, calls=%fused_computation.22 | convolution fusion | flops 1247625216 | bytes 7888896 | tf_op jit(solution)/shard_map/dot_general | solution.py:270
  157.0 20.6 %exchange_dp_5.1 = (bf16[4,48,1536]{2,1,0:T(8,128)(2,1)}, bf16[4,48,1536]{2,1,0:T(8,128)(2,1)}, f32[4,48,128]{2,1,0:T(8,128)}) custom-call(bf16[4,48,1536]{2,1,0:T(8,128)(2,1)} %bitcast.180, bf16[4,48,1536]{2,1,0:T(8,128)(2,1)} %bitcast.179, f32[4,48,128]{2,1,0:T(8,128)} %broadcast_in_dim.20.refs_2_), custom_call_target="tpu_custom_call" | custom-call | tf_op jit(solution)/shard_map/exchange_dp_5/pallas_call | solution.py:62
  177.6 1.2 convert_reduce_fusion.3
  179.8 1.2 convert_reduce_fusion.2
  183.3 10.4 %state_1.1 = (f32[2,48,64,96]{3,2,1,0:T(8,128)}, f32[2,48,64,96]{3,2,1,0:T(8,128)}, f32[48,16,96]{2,1,0:T(8,128)}) custom-call(f32[48,16,96]{2,1,0:T(8,128)} %multiply_bitcast_fusion.u_ref, f32[2,64,96]{2,1,0:T(8,128)} %get-tuple-element.40.are_ref, f32[2,64,96]{2,1,0:T(8,128)} %get-tuple-element.38.aim_ref, ...), custom_call_target="tpu_custom_call", output_to_operand_aliasing={{0}: (9, {}), {1}: (10, {})} | custom-call | tf_op jit(solution)/shard_map/state_1/pallas_call | solution.py:196
  193.7 1.3 fusion.57
  195.4 11.1 %fusion.9 = bf16[48,8448]{1,0:T(8,128)(2,1)S(1)} fusion(bf16[48,1536]{0,1:T(8,128)(2,1)S(1)} %bitcast.176, bf16[2,1536,8448]{2,1,0:T(8,128)(2,1)} %param.19), kind=kOutput, calls=%fused_computation.7 | convolution fusion | flops 1246113792 | bytes 26910720 | tf_op jit(solution)/shard_map/dot_general | solution.py:293
  206.5 1.5 reshape.103
  208.0 1.0 copy.90
  209.0 22.9 %exchange_tp_6.1 = bf16[8,48,1056]{2,1,0:T(8,128)(2,1)} custom-call(bf16[8,48,1056]{2,1,0:T(8,128)(2,1)} %bitcast.168), custom_call_target="tpu_custom_call" | custom-call | tf_op jit(solution)/shard_map/exchange_tp_6/pallas_call | solution.py:62
  232.0 1.3 convert_reduce_fusion
  (48 shorter events, 12.9 us)
Async XLA Ops:
  31.7 6.8 %copy-start.4 = (bf16[2,2112,1536]{2,1,0:T(8,128)(2,1)S(1)}, bf16[2,2112,1536]{2,1,0:T(8,128)(2,1)}, u32[]{:S(2)}) copy-start(bf16[2,2112,1536]{2,1,0:T(8,128)(2,1)} %param.17) | copy-start | bytes 38928388
  61.8 1.5 copy-start.3
  64.1 1.6 copy-start
  94.6 24.8 %copy-start.2 = (bf16[48,1056]{1,0:T(8,128)(2,1)S(1)}, bf16[48,1056]{1,0:T(8,128)(2,1)}, u32[]{:S(2)}) copy-start(bf16[48,1056]{1,0:T(8,128)(2,1)} %x_ref.1) | copy-start | bytes 304132
  209.0 24.3 %copy-start.1 = (bf16[48,1056]{1,0:T(8,128)(2,1)S(1)}, bf16[48,1056]{1,0:T(8,128)(2,1)}, u32[]{:S(2)}) copy-start(bf16[48,1056]{1,0:T(8,128)(2,1)} %add_convert_fusion.1.x_ref) | copy-start | bytes 304132
